TPU v7x, 32 devices: a whole 2x2x4 slice. The times are simulated.
32 devices in a mesh: sp: 8 (over z, y), tp: 4 (over x, core).
Axes of the slice: x: 2, y: 2, z: 4, core: 2. Of those that a mesh axis runs over, the one named last changes fastest.
Arguments:
- residual_in: bfloat16 [6144, 2048], P('sp', 'tp'), may hold values from -11 to 11
- queries: bfloat16 [6144, 1024], P('sp', 'tp'), may hold values from -6 to 6
- keys: bfloat16 [6144, 256], P('sp'), may hold values from -6 to 6
- values: bfloat16 [6144, 256], P('sp'), may hold values from -6 to 6
- query_gain: float32 [128], replicated, may hold values from 1.5 to 5
- key_norm_gain: float32 [128], replicated, may hold values from 1.5 to 5
- out_weight: bfloat16 [1024, 2048], P('tp'), may hold values from -0.1875 to 0.1875
- mlp_gain: float32 [2048], replicated, may hold values from 0.1 to 1.9
- gate_weight: bfloat16 [2048, 5632], P('sp', 'tp'), may hold values from -0.125 to 0.125
- up_weight: bfloat16 [2048, 5632], P('sp', 'tp'), may hold values from -0.125 to 0.125
- down_weight: bfloat16 [5632, 2048], P('tp', 'sp'), may hold values from -0.15625 to 0.15625
Outputs:
- layer_out: bfloat16 [6144, 2048], P('sp', 'tp')
All inputs are finite; a program needn't handle non-finite values.
Results may differ from a plain program's by a relative error of at most 0.012.
The roundings to bfloat16 on the way count: a program that leaves them out, or rounds other values in their place, can miss the bound.
Values may be sent and summed in bfloat16 or wider, within the bound.
No kernel may reach another device: no remote copies, remote signals or barrier semaphores. Data moves between devices by JAX's collectives and lax.ppermute only.
A program may use at most 64 MiB of HBM per device.

v0:
```python
import jax
import jax.numpy as jnp
from jax import lax
from jax.sharding import PartitionSpec as P

D = 2048
HEAD_SIZE = 128
QUERY_HEADS = 8
KEY_VALUE_HEADS = 2
GRID = 64
eps = 1e-06
rotary_base = 10000.0


def apply_rotary(vectors, grid_positions):
    half_size = vectors.shape[-1] // 2
    frequency = rotary_base ** (-jnp.arange(0, half_size, 2, dtype=jnp.float32) / half_size)
    grid_row = (grid_positions // GRID).astype(jnp.float32)
    grid_col = (grid_positions % GRID).astype(jnp.float32)
    angles = jnp.concatenate(
        [grid_row[:, None] * frequency, grid_col[:, None] * frequency], axis=-1
    )[:, None, :]
    cosine_table = jnp.cos(angles)
    sine_table = jnp.sin(angles)
    first_half = vectors[..., :half_size]
    second_half = vectors[..., half_size:]
    return jnp.concatenate(
        [
            first_half * cosine_table - second_half * sine_table,
            first_half * sine_table + second_half * cosine_table,
        ],
        axis=-1,
    )


def per_head_norm(vectors, gain):
    return vectors * lax.rsqrt(jnp.mean(vectors * vectors, axis=-1, keepdims=True) + eps) * gain


def on_device(
    residual_in,
    queries,
    keys,
    values,
    query_gain,
    key_norm_gain,
    out_weight,
    mlp_gain,
    gate_weight,
    up_weight,
    down_weight,
):
    local_rows = residual_in.shape[0]
    local_heads = queries.shape[1] // HEAD_SIZE
    queries_per_group = QUERY_HEADS // KEY_VALUE_HEADS
    tp_index = lax.axis_index("tp")
    grid_positions = lax.axis_index("sp") * local_rows + jnp.arange(local_rows, dtype=jnp.int32)
    query_rows = apply_rotary(
        per_head_norm(
            queries.astype(jnp.float32).reshape(local_rows, local_heads, HEAD_SIZE), query_gain
        ),
        grid_positions,
    ).astype(jnp.bfloat16)
    query_matrix = jnp.transpose(query_rows, (1, 0, 2)).reshape(local_heads * local_rows, HEAD_SIZE)
    shared = tp_index * local_heads // queries_per_group
    own_keys = lax.dynamic_slice_in_dim(keys, shared * HEAD_SIZE, HEAD_SIZE, 1)
    own_values = lax.dynamic_slice_in_dim(values, shared * HEAD_SIZE, HEAD_SIZE, 1)
    key_matrix = apply_rotary(
        per_head_norm(own_keys.astype(jnp.float32)[:, None, :], key_norm_gain), grid_positions
    )[:, 0, :].astype(jnp.bfloat16)
    score_scale = HEAD_SIZE ** (-0.5)
    query_count = local_heads * local_rows
    start_state = (
        jnp.full((query_count,), -1e30, jnp.float32),
        jnp.zeros((query_count,), jnp.float32),
        jnp.zeros((query_count, HEAD_SIZE), jnp.float32),
    )
    key_piece = lax.all_gather(key_matrix, "sp", axis=0, tiled=True)
    value_piece = lax.all_gather(own_values, "sp", axis=0, tiled=True)
    piece_rows = key_piece.shape[0]
    block_count = -(-piece_rows // 2048)
    while piece_rows % block_count:
        block_count += 1
    block_width = piece_rows // block_count

    def one_block(block_index, state_inner):
        running_max, running_sum, weighted = state_inner
        block_keys = lax.dynamic_slice_in_dim(key_piece, block_index * block_width, block_width, 0)
        block_values = lax.dynamic_slice_in_dim(
            value_piece, block_index * block_width, block_width, 0
        )
        scores = (
            jnp.dot(query_matrix, block_keys.T, preferred_element_type=jnp.float32) * score_scale
        )
        new_max = jnp.maximum(running_max, jnp.max(scores, axis=1))
        factor = jnp.exp(running_max - new_max)
        weights = jnp.exp(scores - new_max[:, None])
        running_sum = running_sum * factor + jnp.sum(weights, axis=1)
        weighted = weighted * factor[:, None] + jnp.dot(
            weights.astype(jnp.bfloat16), block_values, preferred_element_type=jnp.float32
        )
        return (new_max, running_sum, weighted)

    running_max, running_sum, weighted = lax.fori_loop(0, block_count, one_block, start_state)
    attended = (weighted / running_sum[:, None]).astype(jnp.bfloat16)
    attended = jnp.transpose(
        attended.reshape(local_heads, local_rows, HEAD_SIZE), (1, 0, 2)
    ).reshape(local_rows, local_heads * HEAD_SIZE)
    own_width = residual_in.shape[1]
    projected = jnp.dot(attended, out_weight, preferred_element_type=jnp.float32).astype(
        jnp.bfloat16
    )
    share = lax.psum_scatter(projected, "tp", scatter_dimension=1, tiled=True).astype(jnp.float32)
    residual_mid = residual_in.astype(jnp.float32) + share
    squares = lax.psum(jnp.sum(residual_mid * residual_mid, axis=1), "tp")
    gain_own = lax.dynamic_slice_in_dim(mlp_gain, tp_index * own_width, own_width, 0)
    normed_own = (residual_mid * lax.rsqrt(squares / D + eps)[:, None] * gain_own).astype(
        jnp.bfloat16
    )
    normed = lax.all_gather(normed_own, "tp", axis=1, tiled=True)
    gate_out = jnp.dot(
        normed,
        lax.all_gather(gate_weight, "sp", axis=0, tiled=True),
        preferred_element_type=jnp.float32,
    )
    up_out = jnp.dot(
        normed,
        lax.all_gather(up_weight, "sp", axis=0, tiled=True),
        preferred_element_type=jnp.float32,
    )
    hidden = (jax.nn.silu(gate_out) * up_out).astype(jnp.bfloat16)
    down_terms = jnp.dot(
        hidden,
        lax.all_gather(down_weight, "sp", axis=1, tiled=True),
        preferred_element_type=jnp.float32,
    )
    down_share = lax.psum_scatter(
        down_terms.astype(jnp.bfloat16), "tp", scatter_dimension=1, tiled=True
    ).astype(jnp.float32)
    return (residual_mid + 0.5 * down_share).astype(jnp.bfloat16)


def solution(mesh):
    in_specs = (
        P("sp", "tp"),
        P("sp", "tp"),
        P("sp", None),
        P("sp", None),
        P(),
        P(),
        P("tp", None),
        P(),
        P("sp", "tp"),
        P("sp", "tp"),
        P("tp", "sp"),
    )
    out_specs = P("sp", "tp")
    return jax.shard_map(
        on_device, mesh=mesh, in_specs=in_specs, out_specs=out_specs, check_vma=False
    )
```

profile of v0, /device:TPU:0, one launch (start us, length us, event | category | flops | bytes accessed | tf_op | source)
XLA Modules:
  0.0 573.1 jit_solution(10254005252952721331)
XLA Ops:
  9.2 1.8 subtract_convert_fusion.1
  12.8 1.4 reshape.236
  14.1 1.7 fusion.18
  17.8 1.4 subtract_convert_fusion
  20.3 38.6 %all-gather.18.cloned.1.call-done = bf16[6144,1,128]{2,0,1:T(8,128)(2,1)} async-done(((bf16[768,1,128]{2,0,1:T(8,128)(2,1)}), bf16[6144,1,128]{2,0,1:T(8,128)(2,1)}) %all-gather.18.cloned.1.call-update) | async-done | bytes 1572880 | tf_op jit(solution)/shard_map/all_gather | solution.py:78
  58.9 44.8 %all-gather.8.cloned.1.call-done = bf16[6144,128]{1,0:T(8,128)(2,1)} async-done(((bf16[768,128]{1,0:T(8,128)(2,1)}), bf16[6144,128]{1,0:T(8,128)(2,1)}) %all-gather.8.cloned.1.call-update) | async-done | bytes 1572880 | tf_op jit(solution)/shard_map/all_gather | solution.py:79
  103.7 57.6 %while.18 = (s32[]{:T(128)}, f32[1536]{0:T(1024)S(1)}, f32[1536]{0:T(1024)S(1)}, f32[1536,128]{1,0:T(8,128)S(1)}, bf16[6144,128]{1,0:T(8,128)(2,1)}, /*index=5*/...) while((s32[]{:T(128)}, f32[1536]{0:T(1024)S(1)}, ...), condition=%wide.region_5.6_spmd.clone, body=%wide.region_2.5_spmd.clone.sunk | while | flops 1636376064 | bytes 91193544 | solution.py:104
  103.7 7.4 %multiply_reduce_fusion.4 = (f32[1536]{0:T(1024)S(1)}, f32[2048,1536]{1,0:T(8,128)}) fusion(bf16[1536,128]{1,0:T(8,128)(2,1)S(1)} %get-tuple-element.266, bf16[6144,128]{1,0:T(8,128)(2,1)} %get-tuple-element.265, s32[]{:T(128)S(6)} %select_n.55), kind=kOutput, calls=%fused_computation.1.clone.1 | convolution fusion | flops 811596288 | bytes 13506564 | tf_op jit(solution)/shard_map/while/body/eval_jaxpr/dot_general | solution.py:93
  111.1 6.8 %fusion.49 = f32[1536]{0:T(1024)S(1)} fusion(f32[2048,1536]{1,0:T(8,128)} %get-tuple-element.236, f32[1536]{0:T(1024)S(1)} %select_maximum_fusion.2), kind=kLoop, calls=%fused_computation.3.clone.1 | loop fusion | flops 9435648 | bytes 12595200 | tf_op jit(solution)/shard_map/while/body/eval_jaxpr/reduce_sum | solution.py:98
  117.9 1.3 copy-done.1
  119.2 3.6 fusion.51
  122.9 7.4 %multiply_reduce_fusion.4 = (f32[1536]{0:T(1024)S(1)}, f32[2048,1536]{1,0:T(8,128)}) fusion(bf16[1536,128]{1,0:T(8,128)(2,1)S(1)} %get-tuple-element.266, bf16[6144,128]{1,0:T(8,128)(2,1)} %get-tuple-element.265, s32[]{:T(128)S(6)} %select_n.55), kind=kOutput, calls=%fused_computation.1.clone.1 | convolution fusion | flops 811596288 | bytes 13506564 | tf_op jit(solution)/shard_map/while/body/eval_jaxpr/dot_general | solution.py:93
  130.3 6.8 %fusion.49 = f32[1536]{0:T(1024)S(1)} fusion(f32[2048,1536]{1,0:T(8,128)} %get-tuple-element.236, f32[1536]{0:T(1024)S(1)} %select_maximum_fusion.2), kind=kLoop, calls=%fused_computation.3.clone.1 | loop fusion | flops 9435648 | bytes 12595200 | tf_op jit(solution)/shard_map/while/body/eval_jaxpr/reduce_sum | solution.py:98
  137.1 1.3 copy-done.1
  138.4 3.6 fusion.51
  142.1 7.4 %multiply_reduce_fusion.4 = (f32[1536]{0:T(1024)S(1)}, f32[2048,1536]{1,0:T(8,128)}) fusion(bf16[1536,128]{1,0:T(8,128)(2,1)S(1)} %get-tuple-element.266, bf16[6144,128]{1,0:T(8,128)(2,1)} %get-tuple-element.265, s32[]{:T(128)S(6)} %select_n.55), kind=kOutput, calls=%fused_computation.1.clone.1 | convolution fusion | flops 811596288 | bytes 13506564 | tf_op jit(solution)/shard_map/while/body/eval_jaxpr/dot_general | solution.py:93
  149.5 6.8 %fusion.49 = f32[1536]{0:T(1024)S(1)} fusion(f32[2048,1536]{1,0:T(8,128)} %get-tuple-element.236, f32[1536]{0:T(1024)S(1)} %select_maximum_fusion.2), kind=kLoop, calls=%fused_computation.3.clone.1 | loop fusion | flops 9435648 | bytes 12595200 | tf_op jit(solution)/shard_map/while/body/eval_jaxpr/reduce_sum | solution.py:98
  156.3 1.3 copy-done.1
  157.6 3.6 fusion.51
  161.8 2.7 convolution_convert_fusion
  166.1 34.7 %reduce-scatter.3.cloned.1.call-done = bf16[768,512]{1,0:T(8,128)(2,1)} async-done(((bf16[768,2048]{1,0:T(8,128)(2,1)}), bf16[768,512]{1,0:T(8,128)(2,1)}) %reduce-scatter.3.cloned.1.call-update) | async-done | bytes 786448 | tf_op jit(solution)/shard_map/reduce_scatter | solution.py:113
  200.8 1.5 multiply_reduce_fusion.1
  202.2 5.8 %psum.7 = f32[768]{0:T(1024)S(1)} all-reduce(f32[768]{0:T(1024)S(1)} %multiply_reduce_fusion.1), channel_id=1, replica_groups=mesh['sp'=8,'tp'=4] {'tp'}, use_global_device_ids=true, to_apply=%region_8.9 | all-reduce | flops 768 | bytes 6144 | tf_op jit(solution)/shard_map/psum | solution.py:115
  208.0 2.3 multiply_convert_fusion.1
  211.7 83.4 %all-gather.12.cloned.1.call-done = bf16[2048,1408]{1,0:T(8,128)(2,1)} async-done(((bf16[256,1408]{1,0:T(8,128)(2,1)}), bf16[2048,1408]{1,0:T(8,128)(2,1)}) %all-gather.12.cloned.1.call-update) | async-done | bytes 5767184 | tf_op jit(solution)/shard_map/all_gather | solution.py:123
  295.1 28.1 %all-gather.10.cloned.1.call-done = bf16[768,2048]{1,0:T(8,128)(2,1)} async-done(((bf16[768,512]{1,0:T(8,128)(2,1)}), bf16[768,2048]{1,0:T(8,128)(2,1)}) %all-gather.10.cloned.1.call-update) | async-done | bytes 3145744 | tf_op jit(solution)/shard_map/all_gather | solution.py:120
  323.3 9.7 %fusion.31 = f32[768,1408]{1,0:T(8,128)} fusion(bf16[768,2048]{1,0:T(8,128)(2,1)} %all-gather.10.cloned.1.call-done, bf16[2048,1408]{1,0:T(8,128)(2,1)} %all-gather.12.cloned.1.call-done), kind=kOutput, calls=%fused_computation.68 | convolution fusion | flops 4429185024 | bytes 13238272 | tf_op jit(solution)/shard_map/dot_general | solution.py:121
  333.0 84.7 %all-gather.14.cloned.1.call-done = bf16[2048,1408]{1,0:T(8,128)(2,1)} async-done(((bf16[256,1408]{1,0:T(8,128)(2,1)}), bf16[2048,1408]{1,0:T(8,128)(2,1)}) %all-gather.14.cloned.1.call-update) | async-done | bytes 5767184 | tf_op jit(solution)/shard_map/all_gather | solution.py:128
  417.6 93.4 %all-gather.16.cloned.1.call-done = bf16[1408,2048]{1,0:T(8,128)(2,1)} async-done(((bf16[1408,256]{1,0:T(8,128)(2,1)}), bf16[1408,2048]{1,0:T(8,128)(2,1)}) %all-gather.16.cloned.1.call-update) | async-done | bytes 5767184 | tf_op jit(solution)/shard_map/all_gather | solution.py:134
  511.0 16.8 %convolution_convert_fusion.1 = bf16[768,2048]{1,0:T(8,128)(2,1)} fusion(bf16[1408,2048]{1,0:T(8,128)(2,1)} %all-gather.16.cloned.1.call-done, f32[768,1408]{1,0:T(8,128)} %fusion.31, bf16[768,2048]{1,0:T(8,128)(2,1)} %all-gather.10.cloned.1.call-done, bf16[2048,1408]{1,0:T(8,128)(2,1)} %all-gather.14.cloned.1.call-done), kind=kOutput, calls=%fused_computation.19 | convolution fusion | flops 8866430976 | bytes 22151168 | tf_op jit(solution)/shard_map/dot_general | solution.py:132
  527.8 36.1 %reduce-scatter.5.cloned.1.call-done = bf16[768,512]{1,0:T(8,128)(2,1)} async-done(((bf16[768,2048]{1,0:T(8,128)(2,1)}), bf16[768,512]{1,0:T(8,128)(2,1)}) %reduce-scatter.5.cloned.1.call-update) | async-done | bytes 786448 | tf_op jit(solution)/shard_map/reduce_scatter | solution.py:137
  563.9 2.3 add_convert_fusion
  (58 shorter events, 10.8 us)
Async XLA Ops:
  6.5 155.2 %copy-start = (bf16[256,2048]{1,0:T(8,128)(2,1)S(1)}, bf16[256,2048]{1,0:T(8,128)(2,1)}, u32[]{:S(2)}) copy-start(bf16[256,2048]{1,0:T(8,128)(2,1)} %param.19) | copy-start | bytes 3145732
  6.5 5.4 copy-start.4
  6.5 52.4 %all-gather.18.cloned.1.call-start = ((), (), s32[]{:S(2)}) async-start(), calls=%async_computation.9 | async-start | bytes 1769472 | tf_op jit(solution)/shard_map/all_gather | solution.py:78
  9.2 7.5 %copy-start.5 = (f32[128]{0:T(128)S(1)}, f32[128]{0:T(128)}, u32[]{:S(2)}) copy-start(f32[128]{0:T(128)} %param.17) | copy-start | bytes 1540
  11.9 91.8 %all-gather.8.cloned.1.call-start = ((), (), s32[]{:S(2)}) async-start(), calls=%async_computation.2 | async-start | bytes 1769472 | tf_op jit(solution)/shard_map/all_gather | solution.py:79
  12.7 188.1 %reduce-scatter.3.cloned.1.call-start = ((), (), s32[]{:S(2)}) async-start(), calls=%async_computation.3 | async-start | bytes 3932160 | tf_op jit(solution)/shard_map/reduce_scatter | solution.py:113
  111.1 8.2 %copy-start.1 = (f32[2048,1536]{1,0:T(8,128)S(1)}, f32[2048,1536]{1,0:T(8,128)}, u32[]{:S(2)}) copy-start(f32[2048,1536]{1,0:T(8,128)} %get-tuple-element.236) | copy-start | bytes 37748740 | tf_op jit(solution)/shard_map/while
  130.3 8.2 %copy-start.1 = (f32[2048,1536]{1,0:T(8,128)S(1)}, f32[2048,1536]{1,0:T(8,128)}, u32[]{:S(2)}) copy-start(f32[2048,1536]{1,0:T(8,128)} %get-tuple-element.236) | copy-start | bytes 37748740 | tf_op jit(solution)/shard_map/while
  149.5 8.2 %copy-start.1 = (f32[2048,1536]{1,0:T(8,128)S(1)}, f32[2048,1536]{1,0:T(8,128)}, u32[]{:S(2)}) copy-start(f32[2048,1536]{1,0:T(8,128)} %get-tuple-element.236) | copy-start | bytes 37748740 | tf_op jit(solution)/shard_map/while
  161.8 39.0 %copy-start.2 = (bf16[768,512]{1,0:T(8,128)(2,1)S(1)}, bf16[768,512]{1,0:T(8,128)(2,1)}, u32[]{:S(2)}) copy-start(bf16[768,512]{1,0:T(8,128)(2,1)} %param.13) | copy-start | bytes 2359300
  164.5 130.6 %all-gather.12.cloned.1.call-start = ((), (), s32[]{:S(2)}) async-start(), calls=%async_computation.5 | async-start | bytes 6488064 | tf_op jit(solution)/shard_map/all_gather | solution.py:123
  165.1 158.2 %all-gather.10.cloned.1.call-start = ((), (), s32[]{:S(2)}) async-start(), calls=%async_computation.4 | async-start | bytes 3932160 | tf_op jit(solution)/shard_map/all_gather | solution.py:120
  210.3 207.3 %all-gather.14.cloned.1.call-start = ((), (), s32[]{:S(2)}) async-start(), calls=%async_computation.6 | async-start | bytes 6488064 | tf_op jit(solution)/shard_map/all_gather | solution.py:128
  210.9 300.1 %all-gather.16.cloned.1.call-start = ((), (), s32[]{:S(2)}) async-start(), calls=%async_computation.7 | async-start | bytes 6488064 | tf_op jit(solution)/shard_map/all_gather | solution.py:134
  211.7 352.2 %reduce-scatter.5.cloned.1.call-start = ((), (), s32[]{:S(2)}) async-start(), calls=%async_computation.8 | async-start | bytes 3932160 | tf_op jit(solution)/shard_map/reduce_scatter | solution.py:137
  333.0 230.9 %copy-start.3 = (bf16[768,512]{1,0:T(8,128)(2,1)S(1)}, bf16[768,512]{1,0:T(8,128)(2,1)}, u32[]{:S(2)}) copy-start(bf16[768,512]{1,0:T(8,128)(2,1)} %reduce-scatter.3.cloned.1.call-done) | copy-start | bytes 2359300
Sparse Core Ops, SparseCore 0:
  12.0 46.8 all-gather.17
  61.1 42.5 all-gather.7
  164.6 36.0 reduce-scatter.2
  202.8 92.2 all-gather.11
  296.5 26.6 all-gather.9
  325.3 92.3 all-gather.13
  419.7 91.2 all-gather.15
  527.9 35.8 reduce-scatter.4
where the time goes:
time: 574 us; the launch traced here: 573 us
  waiting for transfers between devices  446 us (78%)
  matrix products  62.2 us (11%)
  other arithmetic  38.3 us (7%)
  between operations  13.7 us (2%)
  local copies, waits for them, and re-layouts  7.03 us (1%)
  blocking collectives  5.77 us (1%)
    all_gather x1, waiting for transfers between devices, on_device(): lax.all_gather(down_weight, 'sp', axis=1, tiled=True)  93.4 us
    all_gather x1, waiting for transfers between devices, on_device(): lax.all_gather(up_weight, 'sp', axis=0, tiled=True)  84.7 us
    all_gather x1, waiting for transfers between devices, on_device(): lax.all_gather(gate_weight, 'sp', axis=0, tiled=True)  83.4 us
    all_gather x1, waiting for transfers between devices, on_device(): value_piece = lax.all_gather(own_values, 'sp', axis=0, tiled=True)  44.8 us
    all_gather x1, waiting for transfers between devices, on_device(): key_piece = lax.all_gather(key_matrix, 'sp', axis=0, tiled=True)  38.6 us
    reduce_scatter x1, waiting for transfers between devices, on_device(): lax.psum_scatter(down_terms.astype(jnp.bfloat16), 'tp', scatter_dimension...  36.1 us
    reduce_scatter x1, waiting for transfers between devices, on_device(): lax.psum_scatter(projected, 'tp', scatter_dimension=1, tiled=True)  34.7 us
    all_gather x1, waiting for transfers between devices, on_device(): normed = lax.all_gather(normed_own, 'tp', axis=1, tiled=True)  28.1 us
  transfers between devices with their start and end apart: 8, of which 8 were waited for; matrix products, arithmetic and copies ran while one was open for 4% of the time, Pallas kernels for 0%

commit v1 on v0

--- a/solution.py
+++ b/solution.py
@@ -131,7 +131,7 @@
     hidden = (jax.nn.silu(gate_out) * up_out).astype(jnp.bfloat16)
     down_terms = jnp.dot(
         hidden,
-        lax.all_gather(down_weight, "sp", axis=1, tiled=True),
+        jnp.concatenate(lax.all_gather(down_weight, "sp"), axis=1),
         preferred_element_type=jnp.float32,
     )
     down_share = lax.psum_scatter(

time: 574 us -> 573 us (level)
  waiting for transfers between devices: 446 us -> 437 us
  local copies, waits for them, and re-layouts: 7.03 us -> 15.3 us
    all_gather x1, waiting for transfers between devices: 93.4 us -> 84 us  [on_device(): lax.all_gather(down_weight, 'sp')]
    reshape x0 -> x1, local copies, waits for them, and re-layouts: none -> 8.26 us  [on_device(): jnp.concatenate(lax.all_gather(down_weight, 'sp'), axis=1)]
  transfers between devices with their start and end apart: 8 -> 8, of which waited for: 8 -> 8; matrix products, arithmetic and copies ran while one was open for 4% -> 5% of each run, Pallas kernels for 0% -> 0%
where the time goes in v1:
time: 573 us; the launch traced here: 572 us
  waiting for transfers between devices  437 us (76%)
  matrix products  62.2 us (11%)
  other arithmetic  38.3 us (7%)
  local copies, waits for them, and re-layouts  15.3 us (3%)
  between operations  13.7 us (2%)
  blocking collectives  5.77 us (1%)
    all_gather x1, waiting for transfers between devices, on_device(): lax.all_gather(up_weight, 'sp', axis=0, tiled=True)  84.8 us
    all_gather x1, waiting for transfers between devices, on_device(): lax.all_gather(gate_weight, 'sp', axis=0, tiled=True)  84.3 us
    all_gather x1, waiting for transfers between devices, on_device(): lax.all_gather(down_weight, 'sp')  84 us
    all_gather x1, waiting for transfers between devices, on_device(): value_piece = lax.all_gather(own_values, 'sp', axis=0, tiled=True)  44.8 us
    all_gather x1, waiting for transfers between devices, on_device(): key_piece = lax.all_gather(key_matrix, 'sp', axis=0, tiled=True)  38.6 us
    reduce_scatter x1, waiting for transfers between devices, on_device(): lax.psum_scatter(down_terms.astype(jnp.bfloat16), 'tp', scatter_dimension...  36.1 us
    reduce_scatter x1, waiting for transfers between devices, on_device(): lax.psum_scatter(projected, 'tp', scatter_dimension=1, tiled=True)  34.1 us
    all_gather x1, waiting for transfers between devices, on_device(): normed = lax.all_gather(normed_own, 'tp', axis=1, tiled=True)  28.1 us
  transfers between devices with their start and end apart: 8, of which 8 were waited for; matrix products, arithmetic and copies ran while one was open for 5% of the time, Pallas kernels for 0%

profile of v1, /device:TPU:0, one launch (start us, length us, event | category | flops | bytes accessed | tf_op | source)
XLA Modules:
  0.0 572.4 jit_solution(17925022155336443010)
XLA Ops:
  9.2 1.8 subtract_convert_fusion.1
  12.8 1.4 reshape.244
  14.1 1.7 fusion.18
  17.8 1.4 subtract_convert_fusion
  20.3 38.6 %all-gather.17.cloned.1.call-done = bf16[6144,1,128]{2,0,1:T(8,128)(2,1)} async-done(((bf16[768,1,128]{2,0,1:T(8,128)(2,1)}), bf16[6144,1,128]{2,0,1:T(8,128)(2,1)}) %all-gather.17.cloned.1.call-update) | async-done | bytes 1572880 | tf_op jit(solution)/shard_map/all_gather | solution.py:78
  58.9 44.8 %all-gather.9.cloned.1.call-done = bf16[6144,128]{1,0:T(8,128)(2,1)} async-done(((bf16[768,128]{1,0:T(8,128)(2,1)}), bf16[6144,128]{1,0:T(8,128)(2,1)}) %all-gather.9.cloned.1.call-update) | async-done | bytes 1572880 | tf_op jit(solution)/shard_map/all_gather | solution.py:79
  103.7 57.6 %while.18 = (s32[]{:T(128)}, f32[1536]{0:T(1024)S(1)}, f32[1536]{0:T(1024)S(1)}, f32[1536,128]{1,0:T(8,128)S(1)}, bf16[6144,128]{1,0:T(8,128)(2,1)}, /*index=5*/...) while((s32[]{:T(128)}, f32[1536]{0:T(1024)S(1)}, ...), condition=%wide.region_5.6_spmd.clone, body=%wide.region_2.5_spmd.clone.sunk | while | flops 1636376064 | bytes 91193544 | solution.py:104
  103.7 7.4 %multiply_reduce_fusion.4 = (f32[1536]{0:T(1024)S(1)}, f32[2048,1536]{1,0:T(8,128)}) fusion(bf16[1536,128]{1,0:T(8,128)(2,1)S(1)} %get-tuple-element.266, bf16[6144,128]{1,0:T(8,128)(2,1)} %get-tuple-element.265, s32[]{:T(128)S(6)} %select_n.55), kind=kOutput, calls=%fused_computation.1.clone.1 | convolution fusion | flops 811596288 | bytes 13506564 | tf_op jit(solution)/shard_map/while/body/eval_jaxpr/dot_general | solution.py:93
  111.1 6.8 %fusion.49 = f32[1536]{0:T(1024)S(1)} fusion(f32[2048,1536]{1,0:T(8,128)} %get-tuple-element.236, f32[1536]{0:T(1024)S(1)} %select_maximum_fusion.2), kind=kLoop, calls=%fused_computation.3.clone.1 | loop fusion | flops 9435648 | bytes 12595200 | tf_op jit(solution)/shard_map/while/body/eval_jaxpr/reduce_sum | solution.py:98
  119.2 3.6 fusion.51
  122.9 7.4 %multiply_reduce_fusion.4 = (f32[1536]{0:T(1024)S(1)}, f32[2048,1536]{1,0:T(8,128)}) fusion(bf16[1536,128]{1,0:T(8,128)(2,1)S(1)} %get-tuple-element.266, bf16[6144,128]{1,0:T(8,128)(2,1)} %get-tuple-element.265, s32[]{:T(128)S(6)} %select_n.55), kind=kOutput, calls=%fused_computation.1.clone.1 | convolution fusion | flops 811596288 | bytes 13506564 | tf_op jit(solution)/shard_map/while/body/eval_jaxpr/dot_general | solution.py:93
  130.3 6.8 %fusion.49 = f32[1536]{0:T(1024)S(1)} fusion(f32[2048,1536]{1,0:T(8,128)} %get-tuple-element.236, f32[1536]{0:T(1024)S(1)} %select_maximum_fusion.2), kind=kLoop, calls=%fused_computation.3.clone.1 | loop fusion | flops 9435648 | bytes 12595200 | tf_op jit(solution)/shard_map/while/body/eval_jaxpr/reduce_sum | solution.py:98
  137.1 1.3 copy-done.1
  138.4 3.6 fusion.51
  142.1 7.4 %multiply_reduce_fusion.4 = (f32[1536]{0:T(1024)S(1)}, f32[2048,1536]{1,0:T(8,128)}) fusion(bf16[1536,128]{1,0:T(8,128)(2,1)S(1)} %get-tuple-element.266, bf16[6144,128]{1,0:T(8,128)(2,1)} %get-tuple-element.265, s32[]{:T(128)S(6)} %select_n.55), kind=kOutput, calls=%fused_computation.1.clone.1 | convolution fusion | flops 811596288 | bytes 13506564 | tf_op jit(solution)/shard_map/while/body/eval_jaxpr/dot_general | solution.py:93
  149.5 6.8 %fusion.49 = f32[1536]{0:T(1024)S(1)} fusion(f32[2048,1536]{1,0:T(8,128)} %get-tuple-element.236, f32[1536]{0:T(1024)S(1)} %select_maximum_fusion.2), kind=kLoop, calls=%fused_computation.3.clone.1 | loop fusion | flops 9435648 | bytes 12595200 | tf_op jit(solution)/shard_map/while/body/eval_jaxpr/reduce_sum | solution.py:98
  156.3 1.3 copy-done.1
  157.6 3.6 fusion.51
  161.8 2.7 convolution_convert_fusion
  166.7 34.1 %reduce-scatter.3.cloned.1.call-done = bf16[768,512]{1,0:T(8,128)(2,1)} async-done(((bf16[768,2048]{1,0:T(8,128)(2,1)}), bf16[768,512]{1,0:T(8,128)(2,1)}) %reduce-scatter.3.cloned.1.call-update) | async-done | bytes 786448 | tf_op jit(solution)/shard_map/reduce_scatter | solution.py:113
  200.8 1.5 multiply_reduce_fusion.1
  202.2 5.8 %psum.7 = f32[768]{0:T(1024)S(1)} all-reduce(f32[768]{0:T(1024)S(1)} %multiply_reduce_fusion.1), channel_id=1, replica_groups=mesh['sp'=8,'tp'=4] {'tp'}, use_global_device_ids=true, to_apply=%region_8.9 | all-reduce | flops 768 | bytes 6144 | tf_op jit(solution)/shard_map/psum | solution.py:115
  208.0 2.3 multiply_convert_fusion.1
  211.1 84.0 %all-gather.19.cloned.1.call-done = bf16[11264,256]{1,0:T(8,128)(2,1)} async-done(((bf16[1408,256]{1,0:T(8,128)(2,1)}), bf16[11264,256]{1,0:T(8,128)(2,1)}) %all-gather.19.cloned.1.call-update) | async-done | bytes 5767184 | tf_op jit(solution)/shard_map/all_gather | solution.py:134
  295.1 8.3 %copy.24 = bf16[1408,8,256]{0,2,1:T(8,128)(2,1)} copy(bf16[1408,8,256]{2,0,1:T(8,128)(2,1)} %bitcast.29) | data formatting | bytes 11534336 | tf_op jit(solution)/shard_map/reshape | solution.py:134
  303.4 84.3 %all-gather.13.cloned.1.call-done = bf16[2048,1408]{1,0:T(8,128)(2,1)} async-done(((bf16[256,1408]{1,0:T(8,128)(2,1)}), bf16[2048,1408]{1,0:T(8,128)(2,1)}) %all-gather.13.cloned.1.call-update) | async-done | bytes 5767184 | tf_op jit(solution)/shard_map/all_gather | solution.py:123
  387.7 28.1 %all-gather.11.cloned.1.call-done = bf16[768,2048]{1,0:T(8,128)(2,1)} async-done(((bf16[768,512]{1,0:T(8,128)(2,1)}), bf16[768,2048]{1,0:T(8,128)(2,1)}) %all-gather.11.cloned.1.call-update) | async-done | bytes 3145744 | tf_op jit(solution)/shard_map/all_gather | solution.py:120
  415.8 9.7 %fusion.31 = f32[768,1408]{1,0:T(8,128)} fusion(bf16[768,2048]{1,0:T(8,128)(2,1)} %all-gather.11.cloned.1.call-done, bf16[2048,1408]{1,0:T(8,128)(2,1)} %all-gather.13.cloned.1.call-done), kind=kOutput, calls=%fused_computation.68 | convolution fusion | flops 4429185024 | bytes 13238272 | tf_op jit(solution)/shard_map/dot_general | solution.py:121
  425.5 84.8 %all-gather.15.cloned.1.call-done = bf16[2048,1408]{1,0:T(8,128)(2,1)} async-done(((bf16[256,1408]{1,0:T(8,128)(2,1)}), bf16[2048,1408]{1,0:T(8,128)(2,1)}) %all-gather.15.cloned.1.call-update) | async-done | bytes 5767184 | tf_op jit(solution)/shard_map/all_gather | solution.py:128
  510.4 16.8 %convolution_convert_fusion.1 = bf16[768,2048]{1,0:T(8,128)(2,1)} fusion(bf16[1408,2048]{0,1:T(8,128)(2,1)} %bitcast.30, f32[768,1408]{1,0:T(8,128)} %fusion.31, bf16[768,2048]{1,0:T(8,128)(2,1)} %all-gather.11.cloned.1.call-done, bf16[2048,1408]{1,0:T(8,128)(2,1)} %all-gather.15.cloned.1.call-done), kind=kOutput, calls=%fused_computation.19 | convolution fusion | flops 8866430976 | bytes 22151168 | tf_op jit(solution)/shard_map/dot_general | solution.py:132
  527.2 36.1 %reduce-scatter.5.cloned.1.call-done = bf16[768,512]{1,0:T(8,128)(2,1)} async-done(((bf16[768,2048]{1,0:T(8,128)(2,1)}), bf16[768,512]{1,0:T(8,128)(2,1)}) %reduce-scatter.5.cloned.1.call-update) | async-done | bytes 786448 | tf_op jit(solution)/shard_map/reduce_scatter | solution.py:137
  563.2 2.3 add_convert_fusion
  (59 shorter events, 12.1 us)
Async XLA Ops:
  6.5 155.2 %copy-start = (bf16[256,2048]{1,0:T(8,128)(2,1)S(1)}, bf16[256,2048]{1,0:T(8,128)(2,1)}, u32[]{:S(2)}) copy-start(bf16[256,2048]{1,0:T(8,128)(2,1)} %param.19) | copy-start | bytes 3145732
  6.5 5.4 copy-start.4
  6.5 52.4 %all-gather.17.cloned.1.call-start = ((), (), s32[]{:S(2)}) async-start(), calls=%async_computation.8 | async-start | bytes 1769472 | tf_op jit(solution)/shard_map/all_gather | solution.py:78
  9.2 7.5 %copy-start.5 = (f32[128]{0:T(128)S(1)}, f32[128]{0:T(128)}, u32[]{:S(2)}) copy-start(f32[128]{0:T(128)} %param.17) | copy-start | bytes 1540
  11.9 91.8 %all-gather.9.cloned.1.call-start = ((), (), s32[]{:S(2)}) async-start(), calls=%async_computation.2 | async-start | bytes 1769472 | tf_op jit(solution)/shard_map/all_gather | solution.py:79
  12.7 188.1 %reduce-scatter.3.cloned.1.call-start = ((), (), s32[]{:S(2)}) async-start(), calls=%async_computation.3 | async-start | bytes 3932160 | tf_op jit(solution)/shard_map/reduce_scatter | solution.py:113
  111.1 8.2 %copy-start.1 = (f32[2048,1536]{1,0:T(8,128)S(1)}, f32[2048,1536]{1,0:T(8,128)}, u32[]{:S(2)}) copy-start(f32[2048,1536]{1,0:T(8,128)} %get-tuple-element.236) | copy-start | bytes 37748740 | tf_op jit(solution)/shard_map/while
  130.3 8.2 %copy-start.1 = (f32[2048,1536]{1,0:T(8,128)S(1)}, f32[2048,1536]{1,0:T(8,128)}, u32[]{:S(2)}) copy-start(f32[2048,1536]{1,0:T(8,128)} %get-tuple-element.236) | copy-start | bytes 37748740 | tf_op jit(solution)/shard_map/while
  149.5 8.2 %copy-start.1 = (f32[2048,1536]{1,0:T(8,128)S(1)}, f32[2048,1536]{1,0:T(8,128)}, u32[]{:S(2)}) copy-start(f32[2048,1536]{1,0:T(8,128)} %get-tuple-element.236) | copy-start | bytes 37748740 | tf_op jit(solution)/shard_map/while
  161.8 39.0 %copy-start.2 = (bf16[768,512]{1,0:T(8,128)(2,1)S(1)}, bf16[768,512]{1,0:T(8,128)(2,1)}, u32[]{:S(2)}) copy-start(bf16[768,512]{1,0:T(8,128)(2,1)} %param.13) | copy-start | bytes 2359300
  164.5 130.6 %all-gather.19.cloned.1.call-start = ((), (), s32[]{:S(2)}) async-start(), calls=%async_computation.9 | async-start | bytes 6488064 | tf_op jit(solution)/shard_map/all_gather | solution.py:134
  165.1 222.6 %all-gather.13.cloned.1.call-start = ((), (), s32[]{:S(2)}) async-start(), calls=%async_computation.5 | async-start | bytes 6488064 | tf_op jit(solution)/shard_map/all_gather | solution.py:123
  165.7 250.1 %all-gather.11.cloned.1.call-start = ((), (), s32[]{:S(2)}) async-start(), calls=%async_computation.4 | async-start | bytes 3932160 | tf_op jit(solution)/shard_map/all_gather | solution.py:120
  210.3 300.0 %all-gather.15.cloned.1.call-start = ((), (), s32[]{:S(2)}) async-start(), calls=%async_computation.6 | async-start | bytes 6488064 | tf_op jit(solution)/shard_map/all_gather | solution.py:128
  211.1 352.1 %reduce-scatter.5.cloned.1.call-start = ((), (), s32[]{:S(2)}) async-start(), calls=%async_computation.7 | async-start | bytes 3932160 | tf_op jit(solution)/shard_map/reduce_scatter | solution.py:137
  510.4 52.9 %copy-start.3 = (bf16[768,512]{1,0:T(8,128)(2,1)S(1)}, bf16[768,512]{1,0:T(8,128)(2,1)}, u32[]{:S(2)}) copy-start(bf16[768,512]{1,0:T(8,128)(2,1)} %reduce-scatter.3.cloned.1.call-done) | copy-start | bytes 2359300
Sparse Core Ops, SparseCore 0:
  12.0 46.8 all-gather.16
  61.1 42.5 all-gather.8
  164.6 36.0 reduce-scatter.2
  202.8 92.2 all-gather.18
  297.2 90.4 all-gather.12
  389.1 26.6 all-gather.10
  418.0 92.3 all-gather.14
  527.3 35.8 reduce-scatter.4
